TPU v7x, 32 devices: a whole 2x2x4 slice. The times are simulated.
32 devices in a mesh: rep: 2 (over y), fs: 4 (over z), tp: 4 (over x, core).
Axes of the slice: x: 2, y: 2, z: 4, core: 2. Of those that a mesh axis runs over, the one named last changes fastest.
Arguments:
- tokens: bfloat16 [2048, 2048], P(('rep', 'fs')), may hold values from -6 to 6
- gate_weight: bfloat16 [2048, 2816], P('fs', 'tp'), may hold values from -0.125 to 0.125
- up_weight: bfloat16 [2048, 2816], P('fs', 'tp'), may hold values from -0.125 to 0.125
- down_weight: bfloat16 [2816, 2048], P('tp', 'fs'), may hold values from -0.109375 to 0.109375
- out_grad: bfloat16 [2048, 2048], P(('rep', 'fs')), may hold values from -6 to 6
Outputs:
- input_grad: bfloat16 [2048, 2048], P(('rep', 'fs'))
- down_grad: float32 [2816, 2048], P('tp', 'fs')
- row_norms: float32 [2816], P('tp')
All inputs are finite; a program needn't handle non-finite values.
Results may differ from a plain program's by a relative error of at most 0.024.
Values may be sent and summed in bfloat16 or wider, within the bound.
A program may use at most 64 MiB of HBM per device.

v0:
```python
import jax
import jax.numpy as jnp
from jax import lax
from jax.sharding import PartitionSpec as P


def contract_last(left, right):
    return lax.dot_general(
        left, right, (((1,), (1,)), ((), ())), preferred_element_type=jnp.float32
    )


def contract_first(left, right):
    return lax.dot_general(
        left, right, (((0,), (0,)), ((), ())), preferred_element_type=jnp.float32
    )


def on_device(tokens, gate_weight, up_weight, down_weight, out_grad):
    down_full = lax.all_gather(down_weight, "fs", axis=1, tiled=True)
    gate_full, up_full = (
        lax.all_gather(gate_weight, "fs", axis=0, tiled=True),
        lax.all_gather(up_weight, "fs", axis=0, tiled=True),
    )
    gate_pre = jnp.dot(tokens, gate_full, preferred_element_type=jnp.float32)
    up_pre = jnp.dot(tokens, up_full, preferred_element_type=jnp.float32)
    sigma = jax.nn.sigmoid(gate_pre)
    activated = gate_pre * sigma
    hidden = (activated * up_pre).astype(jnp.bfloat16)
    hid_grad = contract_last(out_grad, down_full)
    up_grad = (hid_grad * activated).astype(jnp.bfloat16)
    gate_grad = (hid_grad * up_pre * sigma * (1.0 + gate_pre * (1.0 - sigma))).astype(jnp.bfloat16)
    partial_value = contract_last(gate_grad, gate_full) + contract_last(up_grad, up_full)
    input_grad = lax.psum(partial_value.astype(jnp.bfloat16), "tp")
    columns = lax.all_to_all(out_grad, "fs", split_axis=1, concat_axis=0, tiled=True)
    shard = contract_first(lax.all_gather(hidden, "fs", axis=0, tiled=True), columns)
    shard = lax.psum(shard.astype(jnp.bfloat16), "rep").astype(jnp.float32)
    norms = lax.psum(jnp.sum(shard * shard, axis=1), "fs")
    return (input_grad, shard, norms)


def solution(mesh):
    return jax.shard_map(
        on_device,
        mesh=mesh,
        in_specs=(
            P(("rep", "fs"), None),
            P("fs", "tp"),
            P("fs", "tp"),
            P("tp", "fs"),
            P(("rep", "fs"), None),
        ),
        out_specs=(P(("rep", "fs"), None), P("tp", "fs"), P("tp")),
        check_vma=False,
    )
```

profile of v0, /device:TPU:0, one launch (start us, length us, event | category | flops | bytes accessed | tf_op | source)
XLA Modules:
  0.0 329.1 jit_solution(854777100918134661)
XLA Ops:
  7.2 0.0 copy-start
  7.2 0.0 all-gather.9.cloned.1.call-start
  7.2 0.7 all-gather.9.cloned.1.call-update
  7.9 0.0 all-gather.7.cloned.1.call-start
  8.0 0.7 all-gather.7.cloned.1.call-update
  8.7 0.0 all-gather.5.cloned.1.call-start
  8.7 0.7 all-gather.5.cloned.1.call-update
  9.4 0.0 all-gather.11.cloned.1.call-start
  9.4 62.0 %all-gather.9.cloned.1.call-done = bf16[2048,704]{0,1:T(8,128)(2,1)} async-done(((bf16[512,704]{0,1:T(8,128)(2,1)}), bf16[2048,704]{0,1:T(8,128)(2,1)}) %all-gather.9.cloned.1.call-update) | async-done | bytes 2883600 | tf_op jit(solution)/shard_map/all_gather | solution.py:22
  71.4 0.0 copy-done
  71.4 2.8 fusion.8
  74.2 0.0 copy-start.3
  74.2 0.0 copy-start.2
  74.2 56.6 %all-gather.7.cloned.1.call-done = bf16[2048,704]{0,1:T(8,128)(2,1)} async-done(((bf16[512,704]{0,1:T(8,128)(2,1)}), bf16[2048,704]{0,1:T(8,128)(2,1)}) %all-gather.7.cloned.1.call-update) | async-done | bytes 2883600 | tf_op jit(solution)/shard_map/all_gather | solution.py:23
  130.8 3.7 %multiply_convert_fusion = (bf16[256,704]{0,1:T(8,128)(2,1)}, f32[256,704]{0,1:T(8,128)}) fusion(f32[256,704]{0,1:T(8,128)S(1)} %fusion.8, bf16[256,2048]{1,0:T(8,128)(2,1)S(1)} %copy-done, bf16[2048,704]{0,1:T(8,128)(2,1)} %all-gather.7.cloned.1.call-done), kind=kOutput, calls=%fused_computation.4 | convolution fusion | flops 739278848 | bytes 5734400 | tf_op jit(solution)/shard_map/dot_general | solution.py:26
  134.6 0.0 copy-done.3
  134.6 0.0 all-gather.11.cloned.1.call-update
  134.6 0.0 all-reduce.5.cloned.1.call-start
  134.6 0.0 copy-done.2
  134.7 0.5 copy.8
  135.2 56.6 %all_to_all.19 = bf16[256,4,512]{0,2,1:T(8,128)(2,1)S(1)} all-to-all(bf16[256,4,512]{0,2,1:T(8,128)(2,1)S(1)} %bitcast.14), channel_id=1, replica_groups=mesh['rep'=2,'fs'=4,'tp'=4] {'fs'}, dimensions={1} | all-to-all | bytes 2097152 | tf_op jit(solution)/shard_map/all_to_all | solution.py:35
  191.8 0.5 copy.9
  192.4 17.8 %all-gather.5.cloned.1.call-done = bf16[704,2048]{1,0:T(8,128)(2,1)} async-done(((bf16[704,512]{1,0:T(8,128)(2,1)}), bf16[704,2048]{1,0:T(8,128)(2,1)}) %all-gather.5.cloned.1.call-update) | async-done | bytes 2883600 | tf_op jit(solution)/shard_map/all_gather | solution.py:20
  210.1 3.9 %fusion.7 = f32[256,704]{0,1:T(8,128)} fusion(bf16[256,2048]{1,0:T(8,128)(2,1)} %param.9, bf16[704,2048]{1,0:T(8,128)(2,1)} %all-gather.5.cloned.1.call-done), kind=kOutput, calls=%fused_computation.13 | convolution fusion | flops 738197504 | bytes 4653056 | tf_op jit(solution)/shard_map/dot_general | solution.py:8
  214.1 32.2 %all-gather.11.cloned.1.call-done = bf16[1024,704]{0,1:T(8,128)(2,1)} async-done(((bf16[256,704]{0,1:T(8,128)(2,1)}), bf16[1024,704]{0,1:T(8,128)(2,1)}) %all-gather.11.cloned.1.call-update) | async-done | bytes 1441808 | tf_op jit(solution)/shard_map/all_gather | solution.py:36
  246.3 0.0 copy-start.4
  246.3 3.2 convolution_convert_fusion
  249.5 0.0 all-reduce.5.cloned.1.call-update
  249.5 0.0 all-reduce.3.cloned.1.call-start
  249.6 0.0 copy-done.4
  249.6 0.0 copy-start.1
  249.6 0.0 copy-start.5
  249.6 3.5 %fusion.2 = f32[256,2048]{1,0:T(8,128)S(1)} fusion(bf16[2048,704]{0,1:T(8,128)(2,1)} %all-gather.9.cloned.1.call-done, f32[256,704]{0,1:T(8,128)S(1)} %copy-done.4, f32[256,704]{0,1:T(8,128)} %fusion.7, f32[256,704]{0,1:T(8,128)} %get-tuple-element.6), kind=kOutput, calls=%fused_computation.9 | convolution fusion | flops 739999744 | bytes 7143424 | tf_op jit(solution)/shard_map/dot_general | solution.py:8
  253.1 0.0 copy-done.1
  253.1 0.0 copy-done.5
  253.1 2.0 fusion
  255.2 0.0 all-reduce.3.cloned.1.call-update
  255.2 25.6 %all-reduce.5.cloned.1.call-done = bf16[704,512]{1,0:T(8,128)(2,1)} async-done(((bf16[704,512]{1,0:T(8,128)(2,1)}), bf16[704,512]{1,0:T(8,128)(2,1)}) %all-reduce.5.cloned.1.call-update) | async-done | bytes 720912 | tf_op jit(solution)/shard_map/psum | solution.py:37
  280.8 2.3 multiply_reduce_fusion
  283.1 12.2 %psum.23 = f32[704]{0:T(1024)} all-reduce(f32[704]{0:T(1024)S(1)} %get-tuple-element.3), channel_id=1, replica_groups=mesh['rep'=2,'fs'=4,'tp'=4] {'fs'}, use_global_device_ids=true, to_apply=%region_3.0 | all-reduce | flops 704 | bytes 5632 | tf_op jit(solution)/shard_map/psum | solution.py:38
  295.4 24.5 %all-reduce.3.cloned.1.call-done = bf16[256,2048]{1,0:T(8,128)(2,1)} async-done(((bf16[256,2048]{1,0:T(8,128)(2,1)}), bf16[256,2048]{1,0:T(8,128)(2,1)}) %all-reduce.3.cloned.1.call-update) | async-done | bytes 1048592 | tf_op jit(solution)/shard_map/psum | solution.py:34
  319.9 2.3 copy.12
Async XLA Ops:
  7.2 64.3 %copy-start = (bf16[256,2048]{1,0:T(8,128)(2,1)S(1)}, bf16[256,2048]{1,0:T(8,128)(2,1)}, u32[]{:S(2)}) copy-start(bf16[256,2048]{1,0:T(8,128)(2,1)} %param.5) | copy-start | bytes 3145732
  7.2 64.2 %all-gather.9.cloned.1.call-start = ((), (), s32[]{:S(2)}) async-start(), calls=%async_computation.3 | async-start | bytes 3604480 | tf_op jit(solution)/shard_map/all_gather | solution.py:22
  7.9 122.9 %all-gather.7.cloned.1.call-start = ((), (), s32[]{:S(2)}) async-start(), calls=%async_computation.2 | async-start | bytes 3604480 | tf_op jit(solution)/shard_map/all_gather | solution.py:23
  8.7 201.5 %all-gather.5.cloned.1.call-start = ((), (), s32[]{:S(2)}) async-start(), calls=%async_computation.1 | async-start | bytes 3604480 | tf_op jit(solution)/shard_map/all_gather | solution.py:20
  9.4 236.9 %all-gather.11.cloned.1.call-start = ((), (), s32[]{:S(2)}) async-start(), calls=%async_computation.5 | async-start | bytes 1802240 | tf_op jit(solution)/shard_map/all_gather | solution.py:36
  74.2 60.4 %copy-start.3 = (f32[256,704]{0,1:T(8,128)}, f32[256,704]{0,1:T(8,128)S(1)}, u32[]{:S(2)}) copy-start(f32[256,704]{0,1:T(8,128)S(1)} %fusion.8) | copy-start | bytes 2162692
  74.2 60.4 %copy-start.2 = (bf16[256,2048]{1,0:T(8,128)(2,1)S(1)}, bf16[256,2048]{1,0:T(8,128)(2,1)}, u32[]{:S(2)}) copy-start(bf16[256,2048]{1,0:T(8,128)(2,1)} %param.9) | copy-start | bytes 3145732
  134.6 146.2 %all-reduce.5.cloned.1.call-start = ((), (), s32[]{:S(2)}) async-start(), calls=%async_computation.6 | async-start | bytes 1441792 | tf_op jit(solution)/shard_map/psum | solution.py:37
  246.3 3.3 %copy-start.4 = (f32[256,704]{0,1:T(8,128)S(1)}, f32[256,704]{0,1:T(8,128)}, u32[]{:S(2)}) copy-start(f32[256,704]{0,1:T(8,128)} %copy-done.3) | copy-start | bytes 2162692
  249.5 70.4 %all-reduce.3.cloned.1.call-start = ((), (), s32[]{:S(2)}) async-start(), calls=%async_computation.4 | async-start | bytes 2097152 | tf_op jit(solution)/shard_map/psum | solution.py:34
  249.6 3.5 %copy-start.1 = (bf16[2048,704]{0,1:T(8,128)(2,1)S(1)}, bf16[2048,704]{0,1:T(8,128)(2,1)}, u32[]{:S(2)}) copy-start(bf16[2048,704]{0,1:T(8,128)(2,1)} %all-gather.7.cloned.1.call-done) | copy-start | bytes 8650756
  249.6 3.5 %copy-start.5 = (f32[256,704]{0,1:T(8,128)S(1)}, f32[256,704]{0,1:T(8,128)}, u32[]{:S(2)}) copy-start(f32[256,704]{0,1:T(8,128)} %fusion.7) | copy-start | bytes 2162692
Sparse Core Ops, SparseCore 0:
  9.6 61.8 all-gather.8
  73.0 57.7 all-gather.6
  132.4 77.6 all-gather.4
  211.6 34.6 all-gather.10
  249.6 31.1 all-reduce.4
  283.6 36.2 all-reduce.2
where the time goes:
time: 329 us
  waiting for transfers between devices  221 us (67%)
  blocking collectives  68.9 us (21%)
  matrix products  19.2 us (6%)
  between operations  14.2 us (4%)
  local copies, waits for them, and re-layouts  3.4 us (1%)
    all_gather x1, waiting for transfers between devices, on_device(): lax.all_gather(gate_weight, 'fs', axis=0, tiled=True)  62 us
    all_to_all x1, blocking collectives, on_device(): lax.all_to_all(out_grad, 'fs', split_axis=1, concat_axis=0, tiled=True)  56.6 us
    all_gather x1, waiting for transfers between devices, on_device(): lax.all_gather(up_weight, 'fs', axis=0, tiled=True)  56.6 us
    all_gather x1, waiting for transfers between devices, on_device(): lax.all_gather(hidden, 'fs', axis=0, tiled=True)  32.2 us
    psum x1, waiting for transfers between devices, on_device(): shard = lax.psum(shard.astype(jnp.bfloat16), 'rep').astype(jnp.float32)  25.6 us
    psum x1, waiting for transfers between devices, on_device(): input_grad = lax.psum(partial_value.astype(jnp.bfloat16), 'tp')  24.5 us
    all_gather x1, waiting for transfers between devices, on_device(): down_full = lax.all_gather(down_weight, 'fs', axis=1, tiled=True)  17.8 us
    psum x1, blocking collectives, on_device(): norms = lax.psum(jnp.sum(shard * shard, axis=1), 'fs')  12.2 us
  transfers between devices with their start and end apart: 6, of which 6 were waited for; matrix products, arithmetic and copies ran while one was open for 6% of the time, Pallas kernels for 0%

commit v1 on v0

--- a/solution.py
+++ b/solution.py
@@ -17,7 +17,14 @@
 
 
 def on_device(tokens, gate_weight, up_weight, down_weight, out_grad):
-    down_full = lax.all_gather(down_weight, "fs", axis=1, tiled=True)
+    devices = lax.axis_size("fs")
+    route = [(i, (i + 1) % devices) for i in range(devices)]
+    parts = [down_weight]
+    for reach in range(1, devices):
+        parts = [lax.ppermute(parts[0], "fs", route), *parts]
+    whole = jnp.concatenate(parts, axis=1)
+    offset = (lax.axis_index("fs") + 1) * parts[-1].shape[1]
+    down_full = jnp.roll(whole, offset, axis=1)
     gate_full, up_full = (
         lax.all_gather(gate_weight, "fs", axis=0, tiled=True),
         lax.all_gather(up_weight, "fs", axis=0, tiled=True),

time: 329 us -> 304 us (0.924)
  blocking collectives: 68.9 us -> 12.2 us
  waiting for transfers between devices: 221 us -> 235 us
  starting transfers between devices: 0.24 us -> 13.4 us
  local copies, waits for them, and re-layouts: 3.4 us -> 11.2 us
    all_to_all x1 -> x0, blocking collectives: 56.6 us -> none  [on_device(): lax.all_to_all(out_grad, 'fs', split_axis=1, concat_axis=0, tiled=True)]
    ppermute x0 -> x3, waiting for transfers between devices: none -> 48.1 us  [on_device(): parts = [lax.ppermute(parts[0], 'fs', route), *parts]]
    all_gather x1, waiting for transfers between devices: 32.2 us -> 6.82 us  [on_device(): lax.all_gather(hidden, 'fs', axis=0, tiled=True)]
    all_gather x1 -> x0, waiting for transfers between devices: 17.8 us -> none  [on_device(): down_full = lax.all_gather(down_weight, 'fs', axis=1, tiled=True)]
    ppermute x0 -> x3, starting transfers between devices: none -> 9.4 us  [on_device(): parts = [lax.ppermute(parts[0], 'fs', route), *parts]]
    all_gather x1, waiting for transfers between devices: 62 us -> 71.2 us  [on_device(): lax.all_gather(gate_weight, 'fs', axis=0, tiled=True)]
    unnamed x14 -> x23, local copies, waits for them, and re-layouts: 2.86 us -> 9.82 us
    all_to_all x0 -> x1, starting transfers between devices: none -> 3.86 us  [on_device(): lax.all_to_all(out_grad, 'fs', split_axis=1, concat_axis=0, tiled=True)]
  transfers between devices with their start and end apart: 6 -> 9, of which waited for: 6 -> 7; matrix products, arithmetic and copies ran while one was open for 6% -> 8% of each run, Pallas kernels for 0% -> 0%
where the time goes in v1:
time: 304 us
  waiting for transfers between devices  235 us (77%)
  matrix products  16.1 us (5%)
  between operations  14 us (5%)
  starting transfers between devices  13.4 us (4%)
  blocking collectives  12.2 us (4%)
  local copies, waits for them, and re-layouts  11.2 us (4%)
    all_gather x1, waiting for transfers between devices, on_device(): lax.all_gather(gate_weight, 'fs', axis=0, tiled=True)  71.2 us
    all_gather x1, waiting for transfers between devices, on_device(): lax.all_gather(up_weight, 'fs', axis=0, tiled=True)  56.1 us
    ppermute x3, waiting for transfers between devices, on_device(): parts = [lax.ppermute(parts[0], 'fs', route), *parts]  48.1 us
    psum x1, waiting for transfers between devices, on_device(): shard = lax.psum(shard.astype(jnp.bfloat16), 'rep').astype(jnp.float32)  26.4 us
    psum x1, waiting for transfers between devices, on_device(): input_grad = lax.psum(partial_value.astype(jnp.bfloat16), 'tp')  24.5 us
    psum x1, blocking collectives, on_device(): norms = lax.psum(jnp.sum(shard * shard, axis=1), 'fs')  12.2 us
    unnamed x23, local copies, waits for them, and re-layouts  9.82 us
    ppermute x3, starting transfers between devices, on_device(): parts = [lax.ppermute(parts[0], 'fs', route), *parts]  9.4 us
  transfers between devices with their start and end apart: 9, of which 7 were waited for; matrix products, arithmetic and copies ran while one was open for 8% of the time, Pallas kernels for 0%

profile of v1, /device:TPU:0, one launch (start us, length us, event | category | flops | bytes accessed | tf_op | source)
XLA Modules:
  0.0 303.9 jit_solution(18384705678014434820)
XLA Ops:
  7.2 0.0 copy-start
  7.2 0.0 all-gather.6.cloned.1.call-start
  7.2 0.7 all-gather.6.cloned.1.call-update
  7.9 0.0 all-gather.4.cloned.1.call-start
  8.0 0.7 all-gather.4.cloned.1.call-update
  8.7 3.1 %collective-permute-start = (bf16[704,512]{1,0:T(8,128)(2,1)}, bf16[704,512]{1,0:T(8,128)(2,1)S(1)}, u32[]{:S(2)}, u32[]{:S(2)}) collective-permute-start(bf16[704,512]{1,0:T(8,128)(2,1)} %param.8), channel_id=1, source_target_pairs={{0,4},{4,8},{8,12},{12,0},{1,5},{5,9},{9,13},{13,1},{2,6},{6,10},{... | collective-permute-start | bytes 2162696 | tf_op jit(solution)/shard_map/ppermute | solution.py:24
  11.8 2.3 copy.8
  14.0 3.9 %all-to-all-start = ((bf16[256,4,512]{0,2,1:T(8,128)(2,1)}), bf16[256,4,512]{0,2,1:T(8,128)(2,1)S(1)}, u32[]{:S(2)}, u32[]{:S(2)}) async-start(bf16[256,4,512]{0,2,1:T(8,128)(2,1)} %bitcast.1), calls=%async_computation | async-start | bytes 2097152 | tf_op jit(solution)/shard_map/all_to_all | solution.py:42
  17.9 0.0 all-gather.8.cloned.1.call-start
  17.9 19.4 %collective-permute-done = bf16[704,512]{1,0:T(8,128)(2,1)S(1)} collective-permute-done((bf16[704,512]{1,0:T(8,128)(2,1)}, bf16[704,512]{1,0:T(8,128)(2,1)S(1)}, u32[]{:S(2)}, u32[]{:S(2)}) %collective-permute-start) | collective-permute-done | bytes 720928 | tf_op jit(solution)/shard_map/ppermute | solution.py:24
  37.3 6.2 %collective-permute-start.1 = (bf16[704,512]{1,0:T(8,128)(2,1)S(1)}, bf16[704,512]{1,0:T(8,128)(2,1)}, u32[]{:S(2)}, u32[]{:S(2)}) collective-permute-start(bf16[704,512]{1,0:T(8,128)(2,1)S(1)} %collective-permute-done), channel_id=1, source_target_pairs={{0,4},{4,8},{8,12},{12,0},{1,5},{5,9},{9,13},{13,1},{2,6},{6,10},{... | collective-permute-start | bytes 2162696 | tf_op jit(solution)/shard_map/ppermute | solution.py:24
  43.5 71.2 %all-gather.6.cloned.1.call-done = bf16[2048,704]{0,1:T(8,128)(2,1)} async-done(((bf16[512,704]{0,1:T(8,128)(2,1)}), bf16[2048,704]{0,1:T(8,128)(2,1)}) %all-gather.6.cloned.1.call-update) | async-done | bytes 2883600 | tf_op jit(solution)/shard_map/all_gather | solution.py:29
  114.7 0.0 copy-done
  114.7 2.8 fusion.13
  117.5 0.0 copy-start.5
  117.5 56.1 %all-gather.4.cloned.1.call-done = bf16[2048,704]{0,1:T(8,128)(2,1)} async-done(((bf16[512,704]{0,1:T(8,128)(2,1)}), bf16[2048,704]{0,1:T(8,128)(2,1)}) %all-gather.4.cloned.1.call-update) | async-done | bytes 2883600 | tf_op jit(solution)/shard_map/all_gather | solution.py:30
  173.7 3.7 %multiply_convert_fusion = (bf16[256,704]{0,1:T(8,128)(2,1)}, f32[256,704]{0,1:T(8,128)}) fusion(f32[256,704]{0,1:T(8,128)S(1)} %fusion.13, bf16[256,2048]{1,0:T(8,128)(2,1)S(1)} %copy-done, bf16[2048,704]{0,1:T(8,128)(2,1)} %all-gather.4.cloned.1.call-done), kind=kOutput, calls=%fused_computation.7 | convolution fusion | flops 739278848 | bytes 5734400 | tf_op jit(solution)/shard_map/dot_general | solution.py:33
  177.4 0.0 copy-done.5
  177.4 0.0 all-gather.8.cloned.1.call-update
  177.4 0.0 all-reduce.5.cloned.1.call-start
  177.5 0.0 collective-permute-done.1
  177.5 0.1 collective-permute-start.2
  177.6 0.0 all-to-all-done
  177.6 0.0 copy-start.2
  177.6 1.3 copy.9
  178.9 28.7 %collective-permute-done.2 = bf16[704,512]{1,0:T(8,128)(2,1)} collective-permute-done((bf16[704,512]{1,0:T(8,128)(2,1)}, bf16[704,512]{1,0:T(8,128)(2,1)}, u32[]{:S(2)}, u32[]{:S(2)}) %collective-permute-start.2) | collective-permute-done | bytes 720928 | tf_op jit(solution)/shard_map/ppermute | solution.py:24
  207.6 1.2 constant_dynamic-update-slice_fusion.7
  208.8 1.2 constant_dynamic-update-slice_fusion.6
  210.0 0.1 constant_dynamic-update-slice_fusion.5
  210.1 0.0 copy-done.2
  210.2 0.1 constant_dynamic-update-slice_fusion.4
  210.3 0.0 copy-start.3
  210.3 1.3 constant_dynamic-update-slice_fusion.3
  211.6 1.2 constant_dynamic-update-slice_fusion.2
  212.8 0.1 constant_dynamic-update-slice_fusion.1
  212.9 0.1 constant_dynamic-update-slice_fusion
  213.0 0.0 copy-done.3
  213.0 0.0 copy-start.4
  213.0 0.9 fusion.3
  214.0 6.8 %all-gather.8.cloned.1.call-done = bf16[1024,704]{0,1:T(8,128)(2,1)} async-done(((bf16[256,704]{0,1:T(8,128)(2,1)}), bf16[1024,704]{0,1:T(8,128)(2,1)}) %all-gather.8.cloned.1.call-update) | async-done | bytes 1441808 | tf_op jit(solution)/shard_map/all_gather | solution.py:43
  220.8 0.0 copy-done.4
  220.8 0.0 copy-start.6
  220.8 3.3 %convolution_convert_fusion = bf16[704,512]{1,0:T(8,128)(2,1)} fusion(bf16[1024,704]{0,1:T(8,128)(2,1)} %all-gather.8.cloned.1.call-done, bf16[1024,512]{1,0:T(8,128)(2,1)S(1)} %bitcast.15), kind=kOutput, calls=%fused_computation.5 | convolution fusion | flops 738557952 | bytes 3211264 | tf_op jit(solution)/shard_map/dot_general | solution.py:14
  224.1 0.0 all-reduce.5.cloned.1.call-update
  224.1 0.0 all-reduce.3.cloned.1.call-start
  224.2 0.0 copy-done.6
  224.2 0.0 copy-start.1
  224.2 3.3 %fusion.7 = f32[256,2048]{1,0:T(8,128)S(1)} fusion(bf16[2048,704]{0,1:T(8,128)(2,1)} %all-gather.6.cloned.1.call-done, f32[256,704]{0,1:T(8,128)S(1)} %copy-done.6, f32[256,704]{0,1:T(8,128)S(1)} %fusion.3, f32[256,704]{0,1:T(8,128)} %get-tuple-element.6), kind=kOutput, calls=%fused_computation.12 | convolution fusion | flops 739999744 | bytes 7143424 | tf_op jit(solution)/shard_map/dot_general | solution.py:8
  227.5 0.0 copy-done.1
  227.5 2.0 fusion.2
  229.5 0.0 all-reduce.3.cloned.1.call-update
  229.6 26.4 %all-reduce.5.cloned.1.call-done = bf16[704,512]{1,0:T(8,128)(2,1)} async-done(((bf16[704,512]{1,0:T(8,128)(2,1)}), bf16[704,512]{1,0:T(8,128)(2,1)}) %all-reduce.5.cloned.1.call-update) | async-done | bytes 720912 | tf_op jit(solution)/shard_map/psum | solution.py:44
  255.9 2.3 multiply_reduce_fusion
  258.3 12.2 %psum.23 = f32[704]{0:T(1024)} all-reduce(f32[704]{0:T(1024)S(1)} %get-tuple-element.3), channel_id=1, replica_groups=mesh['rep'=2,'fs'=4,'tp'=4] {'fs'}, use_global_device_ids=true, to_apply=%region_3.4 | all-reduce | flops 704 | bytes 5632 | tf_op jit(solution)/shard_map/psum | solution.py:45
  270.5 24.5 %all-reduce.3.cloned.1.call-done = bf16[256,2048]{1,0:T(8,128)(2,1)} async-done(((bf16[256,2048]{1,0:T(8,128)(2,1)}), bf16[256,2048]{1,0:T(8,128)(2,1)}) %all-reduce.3.cloned.1.call-update) | async-done | bytes 1048592 | tf_op jit(solution)/shard_map/psum | solution.py:41
  295.0 2.3 copy.19
Async XLA Ops:
  7.2 107.6 %copy-start = (bf16[256,2048]{1,0:T(8,128)(2,1)S(1)}, bf16[256,2048]{1,0:T(8,128)(2,1)}, u32[]{:S(2)}) copy-start(bf16[256,2048]{1,0:T(8,128)(2,1)} %param.5) | copy-start | bytes 3145732
  7.2 107.6 %all-gather.6.cloned.1.call-start = ((), (), s32[]{:S(2)}) async-start(), calls=%async_computation.2 | async-start | bytes 3604480 | tf_op jit(solution)/shard_map/all_gather | solution.py:29
  7.9 165.8 %all-gather.4.cloned.1.call-start = ((), (), s32[]{:S(2)}) async-start(), calls=%async_computation.1 | async-start | bytes 3604480 | tf_op jit(solution)/shard_map/all_gather | solution.py:30
  8.7 28.6 %collective-permute-start = (bf16[704,512]{1,0:T(8,128)(2,1)}, bf16[704,512]{1,0:T(8,128)(2,1)S(1)}, u32[]{:S(2)}, u32[]{:S(2)}) collective-permute-start(bf16[704,512]{1,0:T(8,128)(2,1)} %param.8), channel_id=1, source_target_pairs={{0,4},{4,8},{8,12},{12,0},{1,5},{5,9},{9,13},{13,1},{2,6},{6,10},{... | collective-permute-start | bytes 2162696 | tf_op jit(solution)/shard_map/ppermute | solution.py:24
  14.0 163.6 %all-to-all-start = ((bf16[256,4,512]{0,2,1:T(8,128)(2,1)}), bf16[256,4,512]{0,2,1:T(8,128)(2,1)S(1)}, u32[]{:S(2)}, u32[]{:S(2)}) async-start(bf16[256,4,512]{0,2,1:T(8,128)(2,1)} %bitcast.1), calls=%async_computation | async-start | bytes 2097152 | tf_op jit(solution)/shard_map/all_to_all | solution.py:42
  17.9 202.9 %all-gather.8.cloned.1.call-start = ((), (), s32[]{:S(2)}) async-start(), calls=%async_computation.4 | async-start | bytes 1802240 | tf_op jit(solution)/shard_map/all_gather | solution.py:43
  37.3 140.2 %collective-permute-start.1 = (bf16[704,512]{1,0:T(8,128)(2,1)S(1)}, bf16[704,512]{1,0:T(8,128)(2,1)}, u32[]{:S(2)}, u32[]{:S(2)}) collective-permute-start(bf16[704,512]{1,0:T(8,128)(2,1)S(1)} %collective-permute-done), channel_id=1, source_target_pairs={{0,4},{4,8},{8,12},{12,0},{1,5},{5,9},{9,13},{13,1},{2,6},{6,10},{... | collective-permute-start | bytes 2162696 | tf_op jit(solution)/shard_map/ppermute | solution.py:24
  117.5 59.9 %copy-start.5 = (f32[256,704]{0,1:T(8,128)}, f32[256,704]{0,1:T(8,128)S(1)}, u32[]{:S(2)}) copy-start(f32[256,704]{0,1:T(8,128)S(1)} %fusion.13) | copy-start | bytes 2162692
  177.4 78.5 %all-reduce.5.cloned.1.call-start = ((), (), s32[]{:S(2)}) async-start(), calls=%async_computation.5 | async-start | bytes 1441792 | tf_op jit(solution)/shard_map/psum | solution.py:44
  177.5 30.1 %collective-permute-start.2 = (bf16[704,512]{1,0:T(8,128)(2,1)}, bf16[704,512]{1,0:T(8,128)(2,1)}, u32[]{:S(2)}, u32[]{:S(2)}) collective-permute-start(bf16[704,512]{1,0:T(8,128)(2,1)} %collective-permute-done.1), channel_id=1, source_target_pairs={{0,4},{4,8},{8,12},{12,0},{1,5},{5,9},{9,13},{13,1},{2,6},{6,10},{... | collective-permute-start | bytes 2162696 | tf_op jit(solution)/shard_map/ppermute | solution.py:24
  177.6 32.5 %copy-start.2 = (bf16[704,512]{1,0:T(8,128)(2,1)S(1)}, bf16[704,512]{1,0:T(8,128)(2,1)}, u32[]{:S(2)}) copy-start(bf16[704,512]{1,0:T(8,128)(2,1)} %param.8) | copy-start | bytes 2162692
  210.3 2.8 copy-start.3
  213.0 7.8 %copy-start.4 = (bf16[4,256,512]{2,1,0:T(8,128)(2,1)S(1)}, bf16[4,256,512]{2,1,0:T(8,128)(2,1)}, u32[]{:S(2)}) copy-start(bf16[4,256,512]{2,1,0:T(8,128)(2,1)} %copy.9) | copy-start | bytes 3145732
  220.8 3.4 %copy-start.6 = (f32[256,704]{0,1:T(8,128)S(1)}, f32[256,704]{0,1:T(8,128)}, u32[]{:S(2)}) copy-start(f32[256,704]{0,1:T(8,128)} %copy-done.5) | copy-start | bytes 2162692
  224.1 70.9 %all-reduce.3.cloned.1.call-start = ((), (), s32[]{:S(2)}) async-start(), calls=%async_computation.3 | async-start | bytes 2097152 | tf_op jit(solution)/shard_map/psum | solution.py:41
  224.2 3.3 %copy-start.1 = (bf16[2048,704]{0,1:T(8,128)(2,1)S(1)}, bf16[2048,704]{0,1:T(8,128)(2,1)}, u32[]{:S(2)}) copy-start(bf16[2048,704]{0,1:T(8,128)(2,1)} %all-gather.4.cloned.1.call-done) | copy-start | bytes 8650756
Sparse Core Ops, SparseCore 0:
  9.6 105.1 all-gather.5
  116.3 57.3 all-gather.3
  177.6 43.2 all-gather.7
  224.2 31.6 all-reduce.4
  258.7 36.2 all-reduce.2
